TPU v7x, 32 devices: a whole 2x2x4 slice. The times are simulated.
32 devices in a mesh: grp: 2 (over y), fs: 4 (over z), tp: 4 (over x, core).
Axes of the slice: x: 2, y: 2, z: 4, core: 2. Of those that a mesh axis runs over, the one named last changes fastest.
Arguments:
- tokens: bfloat16 [4096, 2048], P(('grp', 'fs'), 'tp'), parts along dimension 0, may hold values from -36 to 36
- query_matrix: bfloat16 [2048, 1024], P('fs', 'tp'), may hold values from -0.125 to 0.125
- key_weight: bfloat16 [2048, 1024], P('fs', 'tp'), may hold values from -0.125 to 0.125
- value_weight: bfloat16 [2048, 2048], P('fs', 'tp'), may hold values from -0.125 to 0.125
- forget_lower_factor: bfloat16 [2048, 32], replicated, may hold values from -0.125 to 0.125
- decay_up: bfloat16 [32, 1024], replicated, may hold values from -1 to 1
- decay_bias: float32 [1024], replicated, may hold values from -1 to 8
- log_extra: float32 [4096, 1024], P(('grp', 'fs'), 'tp'), parts along dimension 0, may hold values from -0.7 to 0
- head_gain: float32 [256], replicated, may hold values from 0.1 to 1.9
- out_weight: bfloat16 [2048, 2048], P('tp', 'fs'), may hold values from -0.125 to 0.125
- mix_gain: float32 [2048], P('tp'), may hold values from 0.1 to 1.9
- up_weight: bfloat16 [2048, 8192], P('fs', 'tp'), may hold values from -0.125 to 0.125
- down_weight: bfloat16 [8192, 2048], P('tp', 'fs'), may hold values from -0.0625 to 0.0625
- out_gain: float32 [2048], P('tp'), may hold values from 0.1 to 1.9
Outputs:
- layer_out: bfloat16 [4096, 2048], P(('grp', 'fs'), 'tp'), parts along dimension 0
There are 2 independent parts, one for each index of `grp`. A program takes and returns all parts, laid end to end along the dimension named above; an argument that names none is the same for every part. Nothing has to cross between parts.
All inputs are finite; a program needn't handle non-finite values.
Results may differ from a plain program's by a relative error of at most 0.015.
Values may be sent and summed in bfloat16 or wider, within the bound.
A program may use at most 64 MiB of HBM per device.

v0:
```python
import jax
import jax.numpy as jnp
from jax import lax
from jax.sharding import PartitionSpec as P

D = 2048
DK = 128
DV = 256
SEGMENT_LENGTH = 64
ALPHA = 2.0**0.5
TAU = 16.0
EPS = 1e-05
HIGH = lax.Precision.HIGHEST


def block_scan(queries, key_rows, value_rows, log_decay):
    span = queries.shape[2]
    causal = (jnp.arange(span)[:, None] >= jnp.arange(span)[None, :])[:, :, None]

    def step(state, inputs):
        query_block, key_block, value_block, decay_block = inputs
        cumul = jnp.cumsum(decay_block, axis=1)
        last_cum = cumul[:, -1:, :]
        carried = jnp.einsum("hcd,hde->hce", query_block * jnp.exp(cumul), state, precision=HIGH)
        differ = cumul[:, :, None, :] - cumul[:, None, :, :]
        weights = jnp.exp(jnp.where(causal, differ, -jnp.inf))
        scores = jnp.sum(query_block[:, :, None, :] * key_block[:, None, :, :] * weights, axis=-1)
        within = jnp.einsum("hij,hje->hie", scores, value_block, precision=HIGH)
        fresh = jnp.einsum(
            "hcd,hce->hde", key_block * jnp.exp(last_cum - cumul), value_block, precision=HIGH
        )
        new_state = jnp.exp(last_cum[:, 0, :])[:, :, None] * state + fresh
        return (new_state, carried + within)

    start = jnp.zeros((queries.shape[1], queries.shape[3], value_rows.shape[3]), jnp.float32)
    _, outputs = lax.scan(step, start, (queries, key_rows, value_rows, log_decay))
    return outputs


def layer_norm(summed, gain_cols):
    row_total, row_squares = lax.psum(
        (jnp.sum(summed, axis=1), jnp.sum(summed * summed, axis=1)), "tp"
    )
    row_mean = row_total / D
    row_var = row_squares / D - row_mean * row_mean
    centered = summed - row_mean[:, None]
    return (centered * lax.rsqrt(row_var[:, None] + EPS) * gain_cols).astype(jnp.bfloat16)


def local(
    tokens,
    query_matrix,
    key_weight,
    value_weight,
    forget_lower_factor,
    decay_up,
    decay_bias,
    log_extra,
    head_gain,
    out_weight,
    mix_gain,
    up_weight,
    down_weight,
    out_gain,
):
    gathered = lax.all_gather(tokens, "tp", axis=1, tiled=True)
    row_count = gathered.shape[0]
    key_cols = query_matrix.shape[1]
    value_cols = value_weight.shape[1]
    local_heads = key_cols // DK
    block_pieces = (
        lax.all_gather(query_matrix, "fs", axis=0, tiled=True),
        lax.all_gather(key_weight, "fs", axis=0, tiled=True),
        lax.all_gather(value_weight, "fs", axis=0, tiled=True),
    )
    columns = gathered
    queries, key_rows, value_rows = tuple(
        (
            jnp.dot(columns, shard_piece, preferred_element_type=jnp.float32)
            for shard_piece in block_pieces
        )
    )
    queries = queries.astype(jnp.bfloat16)
    key_rows = key_rows.astype(jnp.bfloat16)
    value_rows = value_rows.astype(jnp.bfloat16)
    low = jnp.dot(gathered, forget_lower_factor, preferred_element_type=jnp.float32).astype(
        jnp.bfloat16
    )
    offset_cols = lax.axis_index("tp") * key_cols
    local_up = lax.dynamic_slice_in_dim(decay_up, offset_cols, key_cols, 1)
    local_bias = lax.dynamic_slice_in_dim(decay_bias, offset_cols, key_cols, 0)
    gate_pre = jnp.dot(low, local_up, preferred_element_type=jnp.float32) + local_bias
    log_decay = jax.nn.log_sigmoid(gate_pre) / TAU + log_extra
    count = row_count // SEGMENT_LENGTH

    def blocks(array, depth):
        return (
            array.astype(jnp.float32)
            .reshape(count, SEGMENT_LENGTH, local_heads, depth)
            .transpose(0, 2, 1, 3)
        )

    attended = block_scan(
        blocks(queries, DK) * DK ** (-0.5),
        blocks(key_rows, DK),
        blocks(value_rows, DV),
        blocks(log_decay, DK),
    )
    attended = attended.transpose(0, 2, 1, 3).reshape(row_count, local_heads, DV)
    scaled = (
        attended
        * lax.rsqrt(jnp.mean(attended * attended, axis=-1, keepdims=True) + EPS)
        * head_gain
    )
    mixed_heads = scaled.reshape(row_count, value_cols).astype(jnp.bfloat16)
    mix_terms = jnp.dot(
        mixed_heads,
        lax.all_gather(out_weight, "fs", axis=1, tiled=True),
        preferred_element_type=jnp.float32,
    )
    mix = lax.psum_scatter(
        mix_terms.astype(jnp.bfloat16), "tp", scatter_dimension=1, tiled=True
    ).astype(jnp.float32)
    normed_local = layer_norm(ALPHA * tokens.astype(jnp.float32) + mix, mix_gain)
    normed_rows = lax.all_gather(normed_local, "tp", axis=1, tiled=True)
    columns = normed_rows
    hidden = jnp.dot(
        columns,
        lax.all_gather(up_weight, "fs", axis=0, tiled=True),
        preferred_element_type=jnp.float32,
    )
    activation = jnp.square(jax.nn.relu(hidden)).astype(jnp.bfloat16)
    down_terms = jnp.dot(
        activation,
        lax.all_gather(down_weight, "fs", axis=1, tiled=True),
        preferred_element_type=jnp.float32,
    )
    down = lax.psum_scatter(
        down_terms.astype(jnp.bfloat16), "tp", scatter_dimension=1, tiled=True
    ).astype(jnp.float32)
    return layer_norm(ALPHA * normed_local.astype(jnp.float32) + down, out_gain)


def solution(mesh):
    in_specs = (
        P(("grp", "fs"), "tp"),
        P("fs", "tp"),
        P("fs", "tp"),
        P("fs", "tp"),
        P(),
        P(),
        P(),
        P(("grp", "fs"), "tp"),
        P(),
        P("tp", "fs"),
        P("tp"),
        P("fs", "tp"),
        P("tp", "fs"),
        P("tp"),
    )
    out_specs = P(("grp", "fs"), "tp")
    return jax.shard_map(local, mesh=mesh, in_specs=in_specs, out_specs=out_specs, check_vma=False)
```

profile of v0, /device:TPU:0, one launch (start us, length us, event | category | flops | bytes accessed | tf_op | source)
XLA Modules:
  0.0 615.8 jit_solution(9214274555413043903)
XLA Ops:
  10.8 23.4 %all-gather.9.cloned.1.call-done = bf16[512,2048]{1,0:T(8,128)(2,1)} async-done(((bf16[512,512]{1,0:T(8,128)(2,1)}), bf16[512,2048]{1,0:T(8,128)(2,1)}) %all-gather.9.cloned.1.call-update) | async-done | bytes 2097168 | tf_op jit(solution)/shard_map/all_gather | solution.py:66
  34.2 2.8 fusion.31
  37.3 0.9 copy.64
  38.1 25.7 %all-gather.15.cloned.1.call-done = bf16[2048,256]{1,0:T(8,128)(2,1)} async-done(((bf16[512,256]{1,0:T(8,128)(2,1)}), bf16[2048,256]{1,0:T(8,128)(2,1)}) %all-gather.15.cloned.1.call-update) | async-done | bytes 1048592 | tf_op jit(solution)/shard_map/all_gather | solution.py:72
  63.8 2.6 fusion.26
  66.4 1.1 mul.127
  67.4 25.3 %all-gather.11.cloned.1.call-done = bf16[2048,256]{1,0:T(8,128)(2,1)} async-done(((bf16[512,256]{1,0:T(8,128)(2,1)}), bf16[2048,256]{1,0:T(8,128)(2,1)}) %all-gather.11.cloned.1.call-update) | async-done | bytes 1048592 | tf_op jit(solution)/shard_map/all_gather | solution.py:73
  92.8 2.6 fusion.24
  95.3 1.1 reshape.84
  96.4 42.9 %all-gather.13.cloned.1.call-done = bf16[2048,512]{1,0:T(8,128)(2,1)} async-done(((bf16[512,512]{1,0:T(8,128)(2,1)}), bf16[2048,512]{1,0:T(8,128)(2,1)}) %all-gather.13.cloned.1.call-update) | async-done | bytes 2097168 | tf_op jit(solution)/shard_map/all_gather | solution.py:74
  139.3 3.5 fusion.22
  143.6 0.9 copy-done.3
  144.6 0.9 copy_bitcast_fusion.1
  145.6 38.5 %while.13 = (s32[]{:T(128)}, f32[2,128,256]{2,1,0:T(8,128)S(1)}, f32[8,2,64,256]{3,2,1,0:T(8,128)S(1)}, f32[8,2,64,128]{3,2,1,0:T(8,128)}, f32[8,2,64,128]{3,2,1...) while((s32[]{:T(128)}, f32[2,128,256]{2,1,0:T(8,128)S(1)}, ...), condition=%wide.region_3.4_spmd.clone, body=%wide.region_0.3_spmd.clone.sunk | while | flops 132444160 | bytes 2539644 | solution.py:36
  145.6 0.9 dynamic-slice_bitcast_fusion.7
  146.4 0.9 dynamic-slice_bitcast_fusion.6
  147.4 1.9 multiply_reduce_fusion.5
  150.4 0.9 dynamic-slice_bitcast_fusion.7
  151.2 0.9 dynamic-slice_bitcast_fusion.6
  152.2 1.9 multiply_reduce_fusion.5
  155.2 0.9 dynamic-slice_bitcast_fusion.7
  156.1 0.9 dynamic-slice_bitcast_fusion.6
  157.0 1.9 multiply_reduce_fusion.5
  160.0 0.9 dynamic-slice_bitcast_fusion.7
  160.9 0.9 dynamic-slice_bitcast_fusion.6
  161.8 1.9 multiply_reduce_fusion.5
  164.8 0.9 dynamic-slice_bitcast_fusion.7
  165.7 0.9 dynamic-slice_bitcast_fusion.6
  166.7 1.9 multiply_reduce_fusion.5
  169.7 0.9 dynamic-slice_bitcast_fusion.7
  171.5 1.9 multiply_reduce_fusion.5
  174.5 0.9 dynamic-slice_bitcast_fusion.7
  176.3 1.9 multiply_reduce_fusion.5
  179.3 0.9 dynamic-slice_bitcast_fusion.7
  181.1 1.9 multiply_reduce_fusion.5
  186.1 4.2 convolution_convert_fusion.1
  190.4 30.1 %reduce-scatter.3.cloned.1.call-done = bf16[512,512]{1,0:T(8,128)(2,1)} async-done(((bf16[512,2048]{1,0:T(8,128)(2,1)}), bf16[512,512]{1,0:T(8,128)(2,1)}) %reduce-scatter.3.cloned.1.call-update) | async-done | bytes 524304 | tf_op jit(solution)/shard_map/reduce_scatter | solution.py:121
  220.4 1.4 fusion.27
  221.8 5.8 all-reduce.1
  227.6 2.1 multiply_convert_fusion.2
  231.4 21.6 %all-gather.19.cloned.1.call-done = bf16[512,2048]{1,0:T(8,128)(2,1)} async-done(((bf16[512,512]{1,0:T(8,128)(2,1)}), bf16[512,2048]{1,0:T(8,128)(2,1)}) %all-gather.19.cloned.1.call-update) | async-done | bytes 2097168 | tf_op jit(solution)/shard_map/all_gather | solution.py:125
  253.1 151.2 %all-gather.21.cloned.1.call-done = bf16[2048,2048]{1,0:T(8,128)(2,1)} async-done(((bf16[512,2048]{1,0:T(8,128)(2,1)}), bf16[2048,2048]{1,0:T(8,128)(2,1)}) %all-gather.21.cloned.1.call-update) | async-done | bytes 8388624 | tf_op jit(solution)/shard_map/all_gather | solution.py:129
  404.3 149.4 %all-gather.23.cloned.1.call-done = bf16[2048,2048]{1,0:T(8,128)(2,1)} async-done(((bf16[2048,512]{1,0:T(8,128)(2,1)}), bf16[2048,2048]{1,0:T(8,128)(2,1)}) %all-gather.23.cloned.1.call-update) | async-done | bytes 8388624 | tf_op jit(solution)/shard_map/all_gather | solution.py:135
  553.7 16.5 %convolution_convert_fusion = bf16[512,2048]{1,0:T(8,128)(2,1)} fusion(bf16[2048,2048]{1,0:T(8,128)(2,1)} %all-gather.23.cloned.1.call-done, bf16[512,2048]{1,0:T(8,128)(2,1)} %all-gather.19.cloned.1.call-done, bf16[2048,2048]{1,0:T(8,128)(2,1)} %all-gather.21.cloned.1.call-done), kind=kOutput, calls=%fused_computation.29 | convolution fusion | flops 8594128896 | bytes 20971520 | tf_op jit(solution)/shard_map/dot_general | solution.py:133
  570.2 29.5 %reduce-scatter.5.cloned.1.call-done = bf16[512,512]{1,0:T(8,128)(2,1)} async-done(((bf16[512,2048]{1,0:T(8,128)(2,1)}), bf16[512,512]{1,0:T(8,128)(2,1)}) %reduce-scatter.5.cloned.1.call-update) | async-done | bytes 524304 | tf_op jit(solution)/shard_map/reduce_scatter | solution.py:138
  599.7 1.4 fusion.28
  601.1 5.8 all-reduce
  606.9 2.1 multiply_convert_fusion.1
  (114 shorter events, 20.5 us)
Async XLA Ops:
  6.5 27.7 %copy-start = (bf16[2048,32]{0,1:T(8,128)(2,1)S(1)}, bf16[2048,32]{0,1:T(8,128)(2,1)}, u32[]{:S(2)}) copy-start(bf16[2048,32]{0,1:T(8,128)(2,1)} %param.20) | copy-start | bytes 393220
  6.5 3.4 copy-start.7
  6.5 27.7 %copy-start.8 = (f32[512,256]{1,0:T(8,128)S(1)}, f32[512,256]{1,0:T(8,128)}, u32[]{:S(2)}) copy-start(f32[512,256]{1,0:T(8,128)} %param.23) | copy-start | bytes 1572868
  6.5 27.7 %all-gather.9.cloned.1.call-start = ((), (), s32[]{:S(2)}) async-start(), calls=%async_computation.2 | async-start | bytes 2621440 | tf_op jit(solution)/shard_map/all_gather | solution.py:66
  7.3 56.5 %all-gather.15.cloned.1.call-start = ((), (), s32[]{:S(2)}) async-start(), calls=%async_computation.5 | async-start | bytes 1310720 | tf_op jit(solution)/shard_map/all_gather | solution.py:72
  8.0 84.8 %all-gather.11.cloned.1.call-start = ((), (), s32[]{:S(2)}) async-start(), calls=%async_computation.3 | async-start | bytes 1310720 | tf_op jit(solution)/shard_map/all_gather | solution.py:73
  8.7 130.5 %all-gather.13.cloned.1.call-start = ((), (), s32[]{:S(2)}) async-start(), calls=%async_computation.4 | async-start | bytes 2621440 | tf_op jit(solution)/shard_map/all_gather | solution.py:74
  9.3 176.8 %all-gather.17.cloned.1.call-start = ((), (), s32[]{:S(2)}) async-start(), calls=%async_computation.6 | async-start | bytes 2621440 | tf_op jit(solution)/shard_map/all_gather | solution.py:118
  9.9 210.5 %reduce-scatter.3.cloned.1.call-start = ((), (), s32[]{:S(2)}) async-start(), calls=%async_computation.7 | async-start | bytes 2621440 | tf_op jit(solution)/shard_map/reduce_scatter | solution.py:121
  143.4 1.0 copy-start.3
  143.4 1.2 copy-start.4
  190.3 30.1 %copy-start.2 = (bf16[512,512]{1,0:T(8,128)(2,1)S(1)}, bf16[512,512]{1,0:T(8,128)(2,1)}, u32[]{:S(2)}) copy-start(bf16[512,512]{1,0:T(8,128)(2,1)} %param.16) | copy-start | bytes 1572868
  190.3 37.3 %copy-start.5 = (f32[512]{0:T(512)S(1)}, f32[512]{0:T(512)}, u32[]{:S(2)}) copy-start(f32[512]{0:T(512)} %param.26) | copy-start | bytes 6148
  190.3 62.7 %all-gather.19.cloned.1.call-start = ((), (), s32[]{:S(2)}) async-start(), calls=%async_computation.8 | async-start | bytes 2621440 | tf_op jit(solution)/shard_map/all_gather | solution.py:125
  229.7 174.6 %all-gather.21.cloned.1.call-start = ((), (), s32[]{:S(2)}) async-start(), calls=%async_computation.9 | async-start | bytes 10485760 | tf_op jit(solution)/shard_map/all_gather | solution.py:129
  230.5 323.2 %all-gather.23.cloned.1.call-start = ((), (), s32[]{:S(2)}) async-start(), calls=%async_computation.10 | async-start | bytes 10485760 | tf_op jit(solution)/shard_map/all_gather | solution.py:135
  231.2 368.5 %reduce-scatter.5.cloned.1.call-start = ((), (), s32[]{:S(2)}) async-start(), calls=%async_computation.11 | async-start | bytes 2621440 | tf_op jit(solution)/shard_map/reduce_scatter | solution.py:138
  570.2 29.5 %copy-start.1 = (bf16[512,512]{1,0:T(8,128)(2,1)S(1)}, bf16[512,512]{1,0:T(8,128)(2,1)}, u32[]{:S(2)}) copy-start(bf16[512,512]{1,0:T(8,128)(2,1)} %multiply_convert_fusion.2) | copy-start | bytes 1572868
  570.2 36.7 %copy-start.6 = (f32[512]{0:T(512)S(1)}, f32[512]{0:T(512)}, u32[]{:S(2)}) copy-start(f32[512]{0:T(512)} %param.29) | copy-start | bytes 6148
Sparse Core Ops, SparseCore 0:
  8.9 25.2 all-gather.8
  35.8 27.9 all-gather.14
  65.4 27.3 all-gather.10
  94.2 45.0 all-gather.12
  140.7 44.4 all-gather.16
  190.4 29.9 reduce-scatter.2
  229.8 23.1 all-gather.18
  254.6 149.6 all-gather.20
  405.8 147.7 all-gather.22
  570.3 29.3 reduce-scatter.4
where the time goes:
time: 617 us; the launch traced here: 616 us
  waiting for transfers between devices  504 us (82%)
  matrix products  39.9 us (6%)
  other arithmetic  23.6 us (4%)
  local copies, waits for them, and re-layouts  22.3 us (4%)
  between operations  13.7 us (2%)
  blocking collectives  11.5 us (2%)
    all_gather x1, waiting for transfers between devices, local(): lax.all_gather(up_weight, 'fs', axis=0, tiled=True)  151 us
    all_gather x1, waiting for transfers between devices, local(): lax.all_gather(down_weight, 'fs', axis=1, tiled=True)  149 us
    all_gather x1, waiting for transfers between devices, local(): lax.all_gather(value_weight, 'fs', axis=0, tiled=True)  42.9 us
    reduce_scatter x1, waiting for transfers between devices, local(): lax.psum_scatter(mix_terms.astype(jnp.bfloat16), 'tp', scatter_dimension=...  30.1 us
    reduce_scatter x1, waiting for transfers between devices, local(): lax.psum_scatter(down_terms.astype(jnp.bfloat16), 'tp', scatter_dimension...  29.5 us
    all_gather x1, waiting for transfers between devices, local(): lax.all_gather(query_matrix, 'fs', axis=0, tiled=True)  25.7 us
    all_gather x1, waiting for transfers between devices, local(): lax.all_gather(key_weight, 'fs', axis=0, tiled=True)  25.3 us
    all_gather x1, waiting for transfers between devices, local(): gathered = lax.all_gather(tokens, 'tp', axis=1, tiled=True)  23.4 us
  transfers between devices with their start and end apart: 10, of which 9 were waited for; matrix products, arithmetic and copies ran while one was open for 9% of the time, Pallas kernels for 0%

commit v1 on v0

--- a/solution.py
+++ b/solution.py
@@ -11,6 +11,27 @@
 TAU = 16.0
 EPS = 1e-05
 HIGH = lax.Precision.HIGHEST
+
+
+def gather_around(array, axis, dim):
+    peers, index, span = (lax.axis_size(axis), lax.axis_index(axis), array.shape[dim])
+    ahead = [(i, (i + 1) % peers) for i in range(peers)]
+    backward = [(i, (i - 1) % peers) for i in range(peers)]
+    out = jnp.zeros((*array.shape[:dim], peers * span, *array.shape[dim + 1 :]), array.dtype)
+    out = lax.dynamic_update_slice_in_dim(out, array, index * span, axis=dim)
+    from_left = from_right = array
+    half = peers // 2
+    for step in range(1, half + 1):
+        from_left = lax.ppermute(from_left, axis, ahead)
+        out = lax.dynamic_update_slice_in_dim(
+            out, from_left, (index - step) % peers * span, axis=dim
+        )
+        if step < peers - half:
+            from_right = lax.ppermute(from_right, axis, backward)
+            out = lax.dynamic_update_slice_in_dim(
+                out, from_right, (index + step) % peers * span, axis=dim
+            )
+    return out
 
 
 def block_scan(queries, key_rows, value_rows, log_decay):
@@ -131,9 +152,7 @@
     )
     activation = jnp.square(jax.nn.relu(hidden)).astype(jnp.bfloat16)
     down_terms = jnp.dot(
-        activation,
-        lax.all_gather(down_weight, "fs", axis=1, tiled=True),
-        preferred_element_type=jnp.float32,
+        activation, gather_around(down_weight, "fs", 1), preferred_element_type=jnp.float32
     )
     down = lax.psum_scatter(
         down_terms.astype(jnp.bfloat16), "tp", scatter_dimension=1, tiled=True

time: 617 us -> 568 us (0.921)
  waiting for transfers between devices: 504 us -> 403 us
  starting transfers between devices: 0.53 us -> 37.1 us
  local copies, waits for them, and re-layouts: 22.3 us -> 37.5 us
    ppermute x0 -> x3, waiting for transfers between devices: none -> 192 us  [the longest x1 111 us: gather_around(): from_right = lax.ppermute(from_right, axis, backward)]
    all_gather x1 -> x0, waiting for transfers between devices: 149 us -> none  [local(): lax.all_gather(down_weight, 'fs', axis=1, tiled=True)]
    all_gather x1, waiting for transfers between devices: 151 us -> 29.9 us  [local(): lax.all_gather(up_weight, 'fs', axis=0, tiled=True)]
    ppermute x0 -> x3, starting transfers between devices: none -> 36.8 us  [the longest x2 34.7 us: gather_around(): from_left = lax.ppermute(from_left, axis, ahead)]
    all_gather x1, waiting for transfers between devices: 21.6 us -> 0.01 us  [local(): normed_rows = lax.all_gather(normed_local, 'tp', axis=1, tiled=True)]
    dynamic_update_slice x0 -> x4, local copies, waits for them, and re-layouts: none -> 10.9 us  [the longest x2 6.25 us: gather_around(): lax.dynamic_update_slice_in_dim(out, from_left, (index - step) % peers *...]
  transfers between devices with their start and end apart: 10 -> 12, of which waited for: 9 -> 10; matrix products, arithmetic and copies ran while one was open for 9% -> 13% of each run, Pallas kernels for 0% -> 0%
where the time goes in v1:
time: 568 us; the launch traced here: 567 us
  waiting for transfers between devices  403 us (71%)
  matrix products  39.9 us (7%)
  local copies, waits for them, and re-layouts  37.5 us (7%)
  starting transfers between devices  37.1 us (7%)
  other arithmetic  23.8 us (4%)
  between operations  13.4 us (2%)
  blocking collectives  11.5 us (2%)
    ppermute x1, waiting for transfers between devices, gather_around(): from_right = lax.ppermute(from_right, axis, backward)  111 us
    ppermute x2, waiting for transfers between devices, gather_around(): from_left = lax.ppermute(from_left, axis, ahead)  81.7 us
    all_gather x1, waiting for transfers between devices, local(): lax.all_gather(value_weight, 'fs', axis=0, tiled=True)  42.8 us
    ppermute x2, starting transfers between devices, gather_around(): from_left = lax.ppermute(from_left, axis, ahead)  34.7 us
    reduce_scatter x1, waiting for transfers between devices, local(): lax.psum_scatter(mix_terms.astype(jnp.bfloat16), 'tp', scatter_dimension=...  30.1 us
    all_gather x1, waiting for transfers between devices, local(): lax.all_gather(up_weight, 'fs', axis=0, tiled=True)  29.9 us
    reduce_scatter x1, waiting for transfers between devices, local(): lax.psum_scatter(down_terms.astype(jnp.bfloat16), 'tp', scatter_dimension...  29.5 us
    all_gather x1, waiting for transfers between devices, local(): lax.all_gather(query_matrix, 'fs', axis=0, tiled=True)  25.7 us
  transfers between devices with their start and end apart: 12, of which 10 were waited for; matrix products, arithmetic and copies ran while one was open for 13% of the time, Pallas kernels for 0%

profile of v1, /device:TPU:0, one launch (start us, length us, event | category | flops | bytes accessed | tf_op | source)
XLA Modules:
  0.0 566.8 jit_solution(9671313118646140845)
XLA Ops:
  10.8 23.4 %all-gather.8.cloned.1.call-done = bf16[512,2048]{1,0:T(8,128)(2,1)} async-done(((bf16[512,512]{1,0:T(8,128)(2,1)}), bf16[512,2048]{1,0:T(8,128)(2,1)}) %all-gather.8.cloned.1.call-update) | async-done | bytes 2097168 | tf_op jit(solution)/shard_map/all_gather | solution.py:87
  34.2 2.8 fusion.31
  38.1 25.7 %all-gather.14.cloned.1.call-done = bf16[2048,256]{1,0:T(8,128)(2,1)} async-done(((bf16[512,256]{1,0:T(8,128)(2,1)}), bf16[2048,256]{1,0:T(8,128)(2,1)}) %all-gather.14.cloned.1.call-update) | async-done | bytes 1048592 | tf_op jit(solution)/shard_map/all_gather | solution.py:93
  63.8 2.6 fusion.26
  66.4 1.1 mul.139
  67.4 25.3 %all-gather.10.cloned.1.call-done = bf16[2048,256]{1,0:T(8,128)(2,1)} async-done(((bf16[512,256]{1,0:T(8,128)(2,1)}), bf16[2048,256]{1,0:T(8,128)(2,1)}) %all-gather.10.cloned.1.call-update) | async-done | bytes 1048592 | tf_op jit(solution)/shard_map/all_gather | solution.py:94
  92.8 2.6 fusion.24
  95.3 1.1 reshape.84
  96.4 42.8 %all-gather.12.cloned.1.call-done = bf16[2048,512]{1,0:T(8,128)(2,1)} async-done(((bf16[512,512]{1,0:T(8,128)(2,1)}), bf16[2048,512]{1,0:T(8,128)(2,1)}) %all-gather.12.cloned.1.call-update) | async-done | bytes 2097168 | tf_op jit(solution)/shard_map/all_gather | solution.py:95
  139.3 3.5 fusion.22
  143.6 0.9 copy-done.4
  144.6 0.9 copy_bitcast_fusion.1
  145.6 38.5 %while.13 = (s32[]{:T(128)}, f32[2,128,256]{2,1,0:T(8,128)S(1)}, f32[8,2,64,256]{3,2,1,0:T(8,128)S(1)}, f32[8,2,64,128]{3,2,1,0:T(8,128)}, f32[8,2,64,128]{3,2,1...) while((s32[]{:T(128)}, f32[2,128,256]{2,1,0:T(8,128)S(1)}, ...), condition=%wide.region_3.4_spmd.clone, body=%wide.region_0.3_spmd.clone.sunk | while | flops 132444160 | bytes 2540163 | solution.py:57
  146.4 0.9 dynamic-slice_bitcast_fusion.6
  148.2 1.9 multiply_reduce_fusion.5
  150.4 0.9 dynamic-slice_bitcast_fusion.7
  153.0 1.9 multiply_reduce_fusion.5
  155.2 0.9 dynamic-slice_bitcast_fusion.7
  157.8 1.9 multiply_reduce_fusion.5
  162.6 1.9 multiply_reduce_fusion.5
  167.4 1.9 multiply_reduce_fusion.5
  169.7 0.9 dynamic-slice_bitcast_fusion.7
  172.2 1.9 multiply_reduce_fusion.5
  174.5 0.9 dynamic-slice_bitcast_fusion.7
  177.1 1.9 multiply_reduce_fusion.5
  181.9 1.9 multiply_reduce_fusion.5
  186.1 4.2 convolution_convert_fusion.1
  190.4 30.1 %reduce-scatter.3.cloned.1.call-done = bf16[512,512]{1,0:T(8,128)(2,1)} async-done(((bf16[512,2048]{1,0:T(8,128)(2,1)}), bf16[512,512]{1,0:T(8,128)(2,1)}) %reduce-scatter.3.cloned.1.call-update) | async-done | bytes 524304 | tf_op jit(solution)/shard_map/reduce_scatter | solution.py:142
  220.4 1.4 fusion.27
  221.8 5.8 %all-reduce.1 = (f32[512]{0:T(512)S(1)}, f32[512]{0:T(512)S(1)}) all-reduce(f32[512]{0:T(512)S(1)} %get-tuple-element.77, f32[512]{0:T(512)S(1)} %get-tuple-element.76), channel_id=1, replica_groups=mesh['grp'=2,'fs'=4,'tp'=4] {'tp'}, use_global_device_ids=true, to_apply=%region_9.10 | all-reduce | flops 1024 | bytes 8192 | tf_op jit(solution)/shard_map/psum | solution.py:62
  227.6 2.3 multiply_convert_fusion.2
  230.7 1.8 collective-permute-start
  232.4 2.1 collective-permute-start.1
  234.6 58.9 %collective-permute-done = bf16[2048,512]{1,0:T(8,128)(2,1)} collective-permute-done((bf16[2048,512]{1,0:T(8,128)(2,1)S(1)}, bf16[2048,512]{1,0:T(8,128)(2,1)}, u32[]{:S(2)}, u32[]{:S(2)}) %collective-permute-start) | collective-permute-done | bytes 2097184 | tf_op jit(solution)/shard_map/ppermute | solution.py:25
  293.4 32.9 %collective-permute-start.2 = (bf16[2048,512]{1,0:T(8,128)(2,1)}, bf16[2048,512]{1,0:T(8,128)(2,1)}, u32[]{:S(2)}, u32[]{:S(2)}) collective-permute-start(bf16[2048,512]{1,0:T(8,128)(2,1)} %collective-permute-done), channel_id=1, source_target_pairs={{0,4},{4,8},{8,12},{12,0},{1,5},{5,9},{9,13},{13,1},{2,6},{6,10},{... | collective-permute-start | bytes 6291464 | tf_op jit(solution)/shard_map/ppermute | solution.py:25
  326.4 4.3 broadcast_in_dim.29
  330.7 1.5 constant_dynamic-update-slice_fusion.3
  332.2 3.1 constant_dynamic-update-slice_fusion.2
  335.3 110.7 %collective-permute-done.1 = bf16[2048,512]{1,0:T(8,128)(2,1)} collective-permute-done((bf16[2048,512]{1,0:T(8,128)(2,1)S(1)}, bf16[2048,512]{1,0:T(8,128)(2,1)}, u32[]{:S(2)}, u32[]{:S(2)}) %collective-permute-start.1) | collective-permute-done | bytes 2097184 | tf_op jit(solution)/shard_map/ppermute | solution.py:30
  446.0 3.1 constant_dynamic-update-slice_fusion.1
  449.1 22.9 %collective-permute-done.2 = bf16[2048,512]{1,0:T(8,128)(2,1)} collective-permute-done((bf16[2048,512]{1,0:T(8,128)(2,1)}, bf16[2048,512]{1,0:T(8,128)(2,1)}, u32[]{:S(2)}, u32[]{:S(2)}) %collective-permute-start.2) | collective-permute-done | bytes 2097184 | tf_op jit(solution)/shard_map/ppermute | solution.py:25
  472.0 3.1 constant_dynamic-update-slice_fusion
  475.1 29.9 %all-gather.20.cloned.1.call-done = bf16[2048,2048]{1,0:T(8,128)(2,1)} async-done(((bf16[512,2048]{1,0:T(8,128)(2,1)}), bf16[2048,2048]{1,0:T(8,128)(2,1)}) %all-gather.20.cloned.1.call-update) | async-done | bytes 8388624 | tf_op jit(solution)/shard_map/all_gather | solution.py:150
  505.0 16.5 %convolution_convert_fusion = bf16[512,2048]{1,0:T(8,128)(2,1)} fusion(bf16[2048,2048]{1,0:T(8,128)(2,1)} %constant_dynamic-update-slice_fusion, bf16[512,2048]{1,0:T(8,128)(2,1)} %all-gather.18.cloned.1.call-done, bf16[2048,2048]{1,0:T(8,128)(2,1)} %all-gather.20.cloned.1.call-done), kind=kOutput, calls=%fused_computation.29 | convolution fusion | flops 8594128896 | bytes 20971520 | tf_op jit(solution)/shard_map/dot_general | solution.py:154
  521.5 29.5 %reduce-scatter.5.cloned.1.call-done = bf16[512,512]{1,0:T(8,128)(2,1)} async-done(((bf16[512,2048]{1,0:T(8,128)(2,1)}), bf16[512,512]{1,0:T(8,128)(2,1)}) %reduce-scatter.5.cloned.1.call-update) | async-done | bytes 524304 | tf_op jit(solution)/shard_map/reduce_scatter | solution.py:157
  551.0 1.4 fusion.28
  552.3 5.8 %all-reduce = (f32[512]{0:T(512)S(1)}, f32[512]{0:T(512)S(1)}) all-reduce(f32[512]{0:T(512)S(1)} %get-tuple-element.75, f32[512]{0:T(512)S(1)} %get-tuple-element.74), channel_id=1, replica_groups=mesh['grp'=2,'fs'=4,'tp'=4] {'tp'}, use_global_device_ids=true, to_apply=%region_14.15 | all-reduce | flops 1024 | bytes 8192 | tf_op jit(solution)/shard_map/psum | solution.py:62
  558.1 2.1 multiply_convert_fusion.1
  (124 shorter events, 27.2 us)
Async XLA Ops:
  6.5 27.7 %copy-start = (bf16[2048,32]{0,1:T(8,128)(2,1)S(1)}, bf16[2048,32]{0,1:T(8,128)(2,1)}, u32[]{:S(2)}) copy-start(bf16[2048,32]{0,1:T(8,128)(2,1)} %param.20) | copy-start | bytes 393220
  6.5 3.4 copy-start.8
  6.5 27.7 %copy-start.9 = (f32[512,256]{1,0:T(8,128)S(1)}, f32[512,256]{1,0:T(8,128)}, u32[]{:S(2)}) copy-start(f32[512,256]{1,0:T(8,128)} %param.23) | copy-start | bytes 1572868
  6.5 27.7 %all-gather.8.cloned.1.call-start = ((), (), s32[]{:S(2)}) async-start(), calls=%async_computation.2 | async-start | bytes 2621440 | tf_op jit(solution)/shard_map/all_gather | solution.py:87
  7.3 56.5 %all-gather.14.cloned.1.call-start = ((), (), s32[]{:S(2)}) async-start(), calls=%async_computation.5 | async-start | bytes 1310720 | tf_op jit(solution)/shard_map/all_gather | solution.py:93
  8.0 84.8 %all-gather.10.cloned.1.call-start = ((), (), s32[]{:S(2)}) async-start(), calls=%async_computation.3 | async-start | bytes 1310720 | tf_op jit(solution)/shard_map/all_gather | solution.py:94
  8.7 130.5 %all-gather.12.cloned.1.call-start = ((), (), s32[]{:S(2)}) async-start(), calls=%async_computation.4 | async-start | bytes 2621440 | tf_op jit(solution)/shard_map/all_gather | solution.py:95
  9.3 176.8 %all-gather.16.cloned.1.call-start = ((), (), s32[]{:S(2)}) async-start(), calls=%async_computation.6 | async-start | bytes 2621440 | tf_op jit(solution)/shard_map/all_gather | solution.py:139
  9.9 210.5 %reduce-scatter.3.cloned.1.call-start = ((), (), s32[]{:S(2)}) async-start(), calls=%async_computation.7 | async-start | bytes 2621440 | tf_op jit(solution)/shard_map/reduce_scatter | solution.py:142
  143.4 1.0 copy-start.4
  143.4 1.2 copy-start.5
  190.3 30.1 %copy-start.2 = (bf16[512,512]{1,0:T(8,128)(2,1)S(1)}, bf16[512,512]{1,0:T(8,128)(2,1)}, u32[]{:S(2)}) copy-start(bf16[512,512]{1,0:T(8,128)(2,1)} %param.16) | copy-start | bytes 1572868
  190.3 37.3 %copy-start.6 = (f32[512]{0:T(512)S(1)}, f32[512]{0:T(512)}, u32[]{:S(2)}) copy-start(f32[512]{0:T(512)} %param.26) | copy-start | bytes 6148
  190.3 284.8 %all-gather.18.cloned.1.call-start = ((), (), s32[]{:S(2)}) async-start(), calls=%async_computation.8 | async-start | bytes 2621440 | tf_op jit(solution)/shard_map/all_gather | solution.py:146
  227.6 3.1 copy-start.3
  229.9 275.1 %all-gather.20.cloned.1.call-start = ((), (), s32[]{:S(2)}) async-start(), calls=%async_computation.9 | async-start | bytes 10485760 | tf_op jit(solution)/shard_map/all_gather | solution.py:150
  230.6 320.3 %reduce-scatter.5.cloned.1.call-start = ((), (), s32[]{:S(2)}) async-start(), calls=%async_computation.10 | async-start | bytes 2621440 | tf_op jit(solution)/shard_map/reduce_scatter | solution.py:157
  230.7 62.7 %collective-permute-start = (bf16[2048,512]{1,0:T(8,128)(2,1)S(1)}, bf16[2048,512]{1,0:T(8,128)(2,1)}, u32[]{:S(2)}, u32[]{:S(2)}) collective-permute-start(bf16[2048,512]{1,0:T(8,128)(2,1)S(1)} %copy-done.3), channel_id=1, source_target_pairs={{0,4},{4,8},{8,12},{12,0},{1,5},{5,9},{9,13},{13,1},{2,6},{6,10},{... | collective-permute-start | bytes 6291464 | tf_op jit(solution)/shard_map/ppermute | solution.py:25
  232.4 213.5 %collective-permute-start.1 = (bf16[2048,512]{1,0:T(8,128)(2,1)S(1)}, bf16[2048,512]{1,0:T(8,128)(2,1)}, u32[]{:S(2)}, u32[]{:S(2)}) collective-permute-start(bf16[2048,512]{1,0:T(8,128)(2,1)S(1)} %copy-done.3), channel_id=1, source_target_pairs={{0,12},{4,0},{8,4},{12,8},{1,13},{5,1},{9,5},{13,9},{2,14},{6,2},{... | collective-permute-start | bytes 6291464 | tf_op jit(solution)/shard_map/ppermute | solution.py:30
  293.4 178.6 %collective-permute-start.2 = (bf16[2048,512]{1,0:T(8,128)(2,1)}, bf16[2048,512]{1,0:T(8,128)(2,1)}, u32[]{:S(2)}, u32[]{:S(2)}) collective-permute-start(bf16[2048,512]{1,0:T(8,128)(2,1)} %collective-permute-done), channel_id=1, source_target_pairs={{0,4},{4,8},{8,12},{12,0},{1,5},{5,9},{9,13},{13,1},{2,6},{6,10},{... | collective-permute-start | bytes 6291464 | tf_op jit(solution)/shard_map/ppermute | solution.py:25
  521.5 29.5 %copy-start.1 = (bf16[512,512]{1,0:T(8,128)(2,1)S(1)}, bf16[512,512]{1,0:T(8,128)(2,1)}, u32[]{:S(2)}) copy-start(bf16[512,512]{1,0:T(8,128)(2,1)} %multiply_convert_fusion.2) | copy-start | bytes 1572868
  521.5 36.6 %copy-start.7 = (f32[512]{0:T(512)S(1)}, f32[512]{0:T(512)}, u32[]{:S(2)}) copy-start(f32[512]{0:T(512)} %param.29) | copy-start | bytes 6148
Sparse Core Ops, SparseCore 0:
  8.9 25.2 all-gather.7
  35.8 27.9 all-gather.13
  65.4 27.3 all-gather.9
  94.2 45.0 all-gather.11
  140.7 44.4 all-gather.15
  190.5 29.9 reduce-scatter.2
  230.0 23.1 all-gather.17
  254.8 250.1 all-gather.19
  521.6 29.2 reduce-scatter.4
